TPU v7x, 32 devices: a whole 2x2x4 slice. The times are simulated.
32 devices in a mesh: sp: 8 (over z, x), dp: 4 (over y, core).
Axes of the slice: x: 2, y: 2, z: 4, core: 2. Of those that a mesh axis runs over, the one named last changes fastest.
Arguments:
- inputs: bfloat16 [1536, 2048], P('sp'), may hold values from -6 to 6
- w_query: bfloat16 [2048, 2048], P('dp'), may hold values from -0.125 to 0.125
- w_key: bfloat16 [1024, 2048], P('dp'), may hold values from -0.125 to 0.125
- w_value: bfloat16 [1024, 2048], P('dp'), may hold values from -0.125 to 0.125
- query_gain: float32 [64], replicated, may hold values from 0.6 to 7
- key_gain: float32 [64], replicated, may hold values from 0.6 to 7
- grad_out: bfloat16 [1536, 2048], P('sp', 'dp'), may hold values from -6 to 6
Outputs:
- d_inputs: bfloat16 [1536, 2048], P('sp', 'dp')
- grad_wq: float32 [2048, 2048], P('dp')
- grad_wk: float32 [1024, 2048], P('dp')
- grad_wv: float32 [1024, 2048], P('dp')
All inputs are finite; a program needn't handle non-finite values.
Results may differ from a plain program's by a relative error of at most 0.019.
The roundings to bfloat16 on the way count: a program that leaves them out, or rounds other values in their place, can miss the bound.
Values may be sent and summed in bfloat16 or wider, within the bound.
No kernel may reach another device: no remote copies, remote signals or barrier semaphores. Data moves between devices by JAX's collectives and lax.ppermute only.
A program may use at most 64 MiB of HBM per device.

v0:
```python
import jax
import jax.numpy as jnp
from jax import lax
from jax.sharding import PartitionSpec as P

HEAD_WIDTH = 64
GRID_W = 64
norm_eps = 1e-06
axial_base = 10000.0


def rotation_tables(offset, count):
    positions = offset + jnp.arange(count, dtype=jnp.int32)
    grid_rows = (positions // GRID_W).astype(jnp.float32)
    grid_cols = (positions % GRID_W).astype(jnp.float32)
    quarter = HEAD_WIDTH // 4
    freqs_axis = axial_base ** (-jnp.arange(quarter, dtype=jnp.float32) / quarter)
    angle_rows = grid_rows[:, None] * freqs_axis[None, :]
    angle_cols = grid_cols[:, None] * freqs_axis[None, :]
    cosine = jnp.concatenate(
        [jnp.cos(angle_rows), jnp.cos(angle_rows), jnp.cos(angle_cols), jnp.cos(angle_cols)], axis=1
    )
    sine = jnp.concatenate(
        [jnp.sin(angle_rows), jnp.sin(angle_rows), jnp.sin(angle_cols), jnp.sin(angle_cols)], axis=1
    )
    return (cosine, sine)


def quarter_turn(values):
    quarter = HEAD_WIDTH // 4
    return jnp.concatenate(
        [
            -values[..., quarter : 2 * quarter],
            values[..., :quarter],
            -values[..., 3 * quarter :],
            values[..., 2 * quarter : 3 * quarter],
        ],
        axis=-1,
    )


def quarter_back(values):
    quarter = HEAD_WIDTH // 4
    return jnp.concatenate(
        [
            values[..., quarter : 2 * quarter],
            -values[..., :quarter],
            values[..., 3 * quarter :],
            -values[..., 2 * quarter : 3 * quarter],
        ],
        axis=-1,
    )


def rotate(values, cosine, sine):
    return values * cosine + quarter_turn(values) * sine


def rotate_back(grads, cosine, sine):
    return grads * cosine + quarter_back(grads * sine)


def head_norm(raw):
    scale_inv = lax.rsqrt(jnp.mean(raw * raw, axis=-1, keepdims=True) + norm_eps)
    return (raw * scale_inv, scale_inv)


def head_norm_back(grads, normed, scale_inv, gain):
    scaled = grads * gain
    return scale_inv * (scaled - normed * jnp.mean(scaled * normed, axis=-1, keepdims=True))


def body(inputs, w_query, w_key, w_value, query_gain, key_gain, grad_out):
    tok_rows = inputs.shape[0]
    local_query = w_query.shape[0] // HEAD_WIDTH
    local_keys = w_key.shape[0] // HEAD_WIDTH
    group = local_query // local_keys
    key_width = local_keys * HEAD_WIDTH
    scale = HEAD_WIDTH ** (-0.5)
    contract = (((1,), (1,)), ((), ()))
    leading = (((0,), (0,)), ((), ()))
    offset = lax.axis_index("sp") * tok_rows
    cosine, sine = rotation_tables(offset, tok_rows)
    cos_wide = cosine[:, None, :]
    sin_wide = sine[:, None, :]
    q_raw = lax.dot_general(inputs, w_query, contract, preferred_element_type=jnp.float32).astype(
        jnp.bfloat16
    )
    w_pair = jnp.concatenate([w_key, w_value], axis=0)
    kv_raw = lax.dot_general(inputs, w_pair, contract, preferred_element_type=jnp.float32).astype(
        jnp.bfloat16
    )
    q_wide = (
        lax.optimization_barrier(q_raw)
        .astype(jnp.float32)
        .reshape(tok_rows, local_query, HEAD_WIDTH)
    )
    k_wide = (
        lax.optimization_barrier(kv_raw[:, :key_width])
        .astype(jnp.float32)
        .reshape(tok_rows, local_keys, HEAD_WIDTH)
    )
    q_normed, q_inv = head_norm(q_wide)
    k_normed, k_inv = head_norm(k_wide)
    q_rot = rotate(q_normed * query_gain, cos_wide, sin_wide).astype(jnp.bfloat16)
    k_rot = rotate(k_normed * key_gain, cos_wide, sin_wide).astype(jnp.bfloat16)
    kv_rot = jnp.concatenate([k_rot.reshape(tok_rows, key_width), kv_raw[:, key_width:]], axis=1)
    kv_every = lax.all_gather(kv_rot, "sp", axis=0, tiled=True)
    seq_rows = kv_every.shape[0]
    keys_every = kv_every[:, :key_width]
    values_every = kv_every[:, key_width:]
    grad_query = []
    log_totals = []
    deltas = []
    key_terms = [jnp.zeros((seq_rows, HEAD_WIDTH), jnp.float32) for slot in range(local_keys)]
    value_terms = [jnp.zeros((seq_rows, HEAD_WIDTH), jnp.float32) for slot in range(local_keys)]
    for member in range(local_query):
        kv_index = member // group
        query_head = q_rot[:, member, :]
        key_head = keys_every[:, kv_index * HEAD_WIDTH : (kv_index + 1) * HEAD_WIDTH]
        value_head = values_every[:, kv_index * HEAD_WIDTH : (kv_index + 1) * HEAD_WIDTH]
        grad_head = grad_out[:, member * HEAD_WIDTH : (member + 1) * HEAD_WIDTH]
        scores = (
            lax.dot_general(query_head, key_head, contract, preferred_element_type=jnp.float32)
            * scale
        )
        maxima = jnp.max(scores, axis=1, keepdims=True)
        log_total = maxima + jnp.log(jnp.sum(jnp.exp(scores - maxima), axis=1, keepdims=True))
        prob_exact = jnp.exp(scores - log_total)
        prob_half = prob_exact.astype(jnp.bfloat16)
        attn_rows = jnp.dot(prob_half, value_head, preferred_element_type=jnp.float32).astype(
            jnp.bfloat16
        )
        attn_wide = lax.optimization_barrier(attn_rows).astype(jnp.float32)
        delta_rows = jnp.sum(grad_head.astype(jnp.float32) * attn_wide, axis=1, keepdims=True)
        dprob = lax.dot_general(grad_head, value_head, contract, preferred_element_type=jnp.float32)
        dscore = (prob_exact * (dprob - delta_rows)).astype(jnp.bfloat16)
        grad_query.append(jnp.dot(dscore, key_head, preferred_element_type=jnp.float32) * scale)
        log_totals.append(log_total)
        deltas.append(delta_rows)
        value_terms[kv_index] = value_terms[kv_index] + lax.dot_general(
            prob_half, grad_head, leading, preferred_element_type=jnp.float32
        )
        key_terms[kv_index] = (
            key_terms[kv_index]
            + lax.dot_general(dscore, query_head, leading, preferred_element_type=jnp.float32)
            * scale
        )
    gradient_query_rotated = jnp.stack(grad_query, axis=1)
    partial_sums = jnp.concatenate(key_terms + value_terms, axis=1)
    own_grads = lax.psum_scatter(partial_sums, "sp", scatter_dimension=0, tiled=True)
    gradient_key_rotated = own_grads[:, :key_width].reshape(tok_rows, local_keys, HEAD_WIDTH)
    grad_q = head_norm_back(
        rotate_back(gradient_query_rotated, cos_wide, sin_wide), q_normed, q_inv, query_gain
    )
    grad_q = grad_q.reshape(tok_rows, local_query * HEAD_WIDTH).astype(jnp.bfloat16)
    grad_k = head_norm_back(
        rotate_back(gradient_key_rotated, cos_wide, sin_wide), k_normed, k_inv, key_gain
    )
    grad_kv = jnp.concatenate(
        [
            grad_k.reshape(tok_rows, key_width).astype(jnp.bfloat16),
            own_grads[:, key_width:].astype(jnp.bfloat16),
        ],
        axis=1,
    )
    head_part = jnp.dot(grad_q, w_query, preferred_element_type=jnp.float32)
    head_part = head_part + jnp.dot(grad_kv, w_pair, preferred_element_type=jnp.float32)
    d_inputs = lax.psum_scatter(
        head_part.astype(jnp.bfloat16), "dp", scatter_dimension=1, tiled=True
    )
    grad_wq = lax.dot_general(grad_q, inputs, leading, preferred_element_type=jnp.float32)
    grad_wkv = lax.dot_general(grad_kv, inputs, leading, preferred_element_type=jnp.float32)
    grad_wq, grad_wkv = lax.psum((grad_wq, grad_wkv), "sp")
    return (d_inputs, grad_wq, grad_wkv[:key_width], grad_wkv[key_width:])


def solution(mesh):
    return jax.shard_map(
        body,
        mesh=mesh,
        in_specs=(
            P("sp", None),
            P("dp", None),
            P("dp", None),
            P("dp", None),
            P(),
            P(),
            P("sp", "dp"),
        ),
        out_specs=(P("sp", "dp"), P("dp", None), P("dp", None), P("dp", None)),
        check_vma=False,
    )
```

profile of v0, /device:TPU:0, one launch (start us, length us, event | category | flops | bytes accessed | tf_op | source)
XLA Modules:
  0.0 498.9 jit_solution(4581374337283304342)
XLA Ops:
  9.1 1.4 constant_dynamic-update-slice_fusion.1
  16.6 1.7 copy.97
  21.3 1.6 pad_maximum_fusion.1
  22.9 1.5 convolution_convert_fusion.1
  25.2 1.5 copy.126
  26.7 1.5 copy.125
  34.6 35.3 %all-gather.2.cloned.1.call-done = bf16[1536,512]{1,0:T(8,128)(2,1)} async-done(((bf16[192,512]{1,0:T(8,128)(2,1)}), bf16[1536,512]{1,0:T(8,128)(2,1)}) %all-gather.2.cloned.1.call-update) | async-done | bytes 1572880 | tf_op jit(solution)/shard_map/all_gather | solution.py:108
  69.9 1.6 fusion.148
  95.9 1.1 fusion.28
  97.1 1.1 fusion.27
  100.5 3.5 copy.117
  106.2 2.0 copy.109
  108.3 1.6 fusion.53
  109.9 1.6 fusion.51
  111.5 1.7 fusion.49
  116.6 1.6 multiply_reduce_fusion
  118.2 2.0 copy.106
  121.8 1.4 multiply_convert_fusion
  123.2 2.8 fusion.156
  126.0 51.0 %reduce-scatter.7.cloned.1.call-done = f32[192,512]{1,0:T(8,128)} async-done(((f32[1536,512]{1,0:T(8,128)}), f32[192,512]{1,0:T(8,128)}) %reduce-scatter.7.cloned.1.call-update) | async-done | bytes 393232 | tf_op jit(solution)/shard_map/reduce_scatter | solution.py:151
  177.0 1.6 slice.233
  178.6 1.8 copy.112
  181.5 1.6 pad_maximum_fusion
  183.1 1.8 copy.113
  185.7 1.7 copy.114
  188.4 1.3 multiply_convert_fusion.1
  190.3 2.7 fusion.96
  194.8 1.5 fusion.16
  196.3 266.0 %all-reduce.3.cloned.1.call-done = (f32[512,2048]{1,0:T(8,128)}, f32[512,2048]{1,0:T(8,128)}) async-done(((f32[512,2048]{1,0:T(8,128)}, f32[512,2048]{1,0:T(8,128)}), (f32[512,2048]{1,0:T(8,128)}, f32[512,2048]{1,0:T(8,128)})) %all-reduce.3.cloned.1.call-update) | async-done | bytes 8388624 | tf_op jit(solution)/shard_map/psum | solution.py:174
  462.3 4.7 fusion.142
  467.0 20.6 %reduce-scatter.5.cloned.1.call-done = bf16[192,512]{1,0:T(8,128)(2,1)} async-done(((bf16[192,2048]{1,0:T(8,128)(2,1)}), bf16[192,512]{1,0:T(8,128)(2,1)}) %reduce-scatter.5.cloned.1.call-update) | async-done | bytes 196624 | tf_op jit(solution)/shard_map/reduce_scatter | solution.py:169
  487.7 4.7 copy.144
  (222 shorter events, 56.7 us)
Async XLA Ops:
  7.2 15.8 %copy-start = (bf16[512,2048]{1,0:T(8,128)(2,1)S(1)}, bf16[512,2048]{1,0:T(8,128)(2,1)}, u32[]{:S(2)}) copy-start(bf16[512,2048]{1,0:T(8,128)(2,1)} %param.8) | copy-start | bytes 6291460
  7.2 62.7 %all-gather.2.cloned.1.call-start = ((), (), s32[]{:S(2)}) async-start(), calls=%async_computation.2 | async-start | bytes 1769472 | tf_op jit(solution)/shard_map/all_gather | solution.py:108
  8.1 12.0 %copy-start.43 = (f32[256]{0:T(256)}, f32[256]{0:T(256)S(1)}, u32[]{:S(2)}) copy-start(f32[256]{0:T(256)S(1)} %mul.354) | copy-start | bytes 3076
  9.0 107.1 %copy-start.29 = (f32[192,64]{0,1:T(8,128)}, f32[192,64]{0,1:T(8,128)S(1)}, u32[]{:S(2)}) copy-start(f32[192,64]{0,1:T(8,128)S(1)} %pad_maximum_fusion.5) | copy-start | bytes 147460
  9.1 11.0 %copy-start.25 = (f32[192,256]{1,0:T(8,128)}, f32[192,256]{1,0:T(8,128)S(1)}, u32[]{:S(2)}) copy-start(f32[192,256]{1,0:T(8,128)S(1)} %copy.96) | copy-start | bytes 589828
  9.1 1.6 copy-start.30
  10.7 1.1 copy-start.3
  11.9 1.3 copy-start.19
  11.9 3.1 copy-start.48
  14.9 3.5 copy-start.21
  20.1 2.7 copy-start.27
  22.9 1.6 copy-start.4
  22.9 154.1 %reduce-scatter.7.cloned.1.call-start = ((), (), s32[]{:S(2)}) async-start(), calls=%async_computation.4 | async-start | bytes 3538944 | tf_op jit(solution)/shard_map/reduce_scatter | solution.py:151
  24.5 9.1 %copy-start.45 = (f32[64]{0:T(128)S(1)}, f32[64]{0:T(128)}, u32[]{:S(2)}) copy-start(f32[64]{0:T(128)} %param.11) | copy-start | bytes 772
  69.9 1.9 copy-start.1
  94.9 2.1 copy-start.12
  104.0 358.3 %all-reduce.3.cloned.1.call-start = ((), (), s32[]{:S(2)}) async-start(), calls=%async_computation.5 | async-start | bytes 16777216 | tf_op jit(solution)/shard_map/psum | solution.py:174
  108.3 3.2 copy-start.2
  109.9 3.3 copy-start.17
  111.5 2.2 copy-start.9
  113.7 1.1 copy-start.7
  114.2 1.1 copy-start.13
  118.1 3.7 copy-start.47
  126.0 55.5 %copy-start.22 = (f32[192,256]{0,1:T(8,128)S(1)}, f32[192,256]{0,1:T(8,128)}, u32[]{:S(2)}) copy-start(f32[192,256]{0,1:T(8,128)} %copy-done.21) | copy-start | bytes 589828
  126.0 55.5 %copy-start.49 = (f32[64]{0:T(128)S(1)}, f32[64]{0:T(128)}, u32[]{:S(2)}) copy-start(f32[64]{0:T(128)} %param.12) | copy-start | bytes 772
  180.4 1.1 copy-start.24
  181.5 6.8 %copy-start.26 = (f32[192,256]{1,0:T(8,128)S(1)}, f32[192,256]{1,0:T(8,128)}, u32[]{:S(2)}) copy-start(f32[192,256]{1,0:T(8,128)} %copy-done.25) | copy-start | bytes 589828
  181.5 6.8 %copy-start.44 = (f32[256]{0:T(256)S(1)}, f32[256]{0:T(256)}, u32[]{:S(2)}) copy-start(f32[256]{0:T(256)} %copy-done.43) | copy-start | bytes 3076
  183.1 5.2 %copy-start.28 = (f32[192,256]{1,0:T(8,128)S(1)}, f32[192,256]{1,0:T(8,128)}, u32[]{:S(2)}) copy-start(f32[192,256]{1,0:T(8,128)} %copy-done.27) | copy-start | bytes 589828
  188.4 1.3 copy-start.31
  193.1 294.6 %reduce-scatter.5.cloned.1.call-start = ((), (), s32[]{:S(2)}) async-start(), calls=%async_computation.3 | async-start | bytes 983040 | tf_op jit(solution)/shard_map/reduce_scatter | solution.py:169
  193.1 1.6 copy-start.20
  (22 other events, 18.5 us)
Sparse Core Ops, SparseCore 0:
  23.0 46.8 all-gather.1
  104.2 72.8 reduce-scatter.6
  193.2 269.0 all-reduce.2
  465.3 22.3 reduce-scatter.4
where the time goes:
time: 500 us; the launch traced here: 499 us
  waiting for transfers between devices  373 us (75%)
  local copies, waits for them, and re-layouts  54.1 us (11%)
  matrix products  40.2 us (8%)
  other arithmetic  16.9 us (3%)
  between operations  14.6 us (3%)
    psum x1, waiting for transfers between devices, body(): grad_wq, grad_wkv = lax.psum((grad_wq, grad_wkv), 'sp')  266 us
    reduce_scatter x1, waiting for transfers between devices, body(): lax.psum_scatter(partial_sums, 'sp', scatter_dimension=0, tiled=True)  51 us
    all_gather x1, waiting for transfers between devices, body(): kv_every = lax.all_gather(kv_rot, 'sp', axis=0, tiled=True)  35.3 us
    unnamed x112, local copies, waits for them, and re-layouts  26.3 us
    reduce_scatter x1, waiting for transfers between devices, body(): lax.psum_scatter(head_part.astype(jnp.bfloat16), 'dp', scatter_dimension=...  20.6 us
  transfers between devices with their start and end apart: 4, of which 4 were waited for; matrix products, arithmetic and copies ran while one was open for 8% of the time, Pallas kernels for 0%

commit v1 on v0

--- a/solution.py
+++ b/solution.py
@@ -105,7 +105,12 @@
     q_rot = rotate(q_normed * query_gain, cos_wide, sin_wide).astype(jnp.bfloat16)
     k_rot = rotate(k_normed * key_gain, cos_wide, sin_wide).astype(jnp.bfloat16)
     kv_rot = jnp.concatenate([k_rot.reshape(tok_rows, key_width), kv_raw[:, key_width:]], axis=1)
-    kv_every = lax.all_gather(kv_rot, "sp", axis=0, tiled=True)
+    ring = [kv_rot]
+    for hop in range(7):
+        ring.append(lax.ppermute(ring[-1], "sp", [(dev, (dev + 1) % 8) for dev in range(8)]))
+    kv_every = jnp.roll(
+        jnp.concatenate(ring[::-1], axis=0), (lax.axis_index("sp") + 1) * ring[0].shape[0], axis=0
+    )
     seq_rows = kv_every.shape[0]
     keys_every = kv_every[:, :key_width]
     values_every = kv_every[:, key_width:]

time: 500 us -> 517 us (1.034)
  waiting for transfers between devices: 373 us -> 386 us
    ppermute x0 -> x7, waiting for transfers between devices: none -> 51.2 us  [body(): lax.ppermute(ring[-1], 'sp', [(dev, (dev + 1) % 8) for dev in range(8)])]
    all_gather x1 -> x0, waiting for transfers between devices: 35.3 us -> none  [body(): kv_every = lax.all_gather(kv_rot, 'sp', axis=0, tiled=True)]
    unnamed x112 -> x132, local copies, waits for them, and re-layouts: 26.3 us -> 25.3 us
  transfers between devices with their start and end apart: 4 -> 10, of which waited for: 4 -> 10; matrix products, arithmetic and copies ran while one was open for 8% -> 7% of each run, Pallas kernels for 0% -> 0%
where the time goes in v1:
time: 517 us; the launch traced here: 516 us
  waiting for transfers between devices  386 us (75%)
  local copies, waits for them, and re-layouts  53 us (10%)
  matrix products  42.6 us (8%)
  other arithmetic  15.5 us (3%)
  between operations  14.8 us (3%)
    psum x1, waiting for transfers between devices, body(): grad_wq, grad_wkv = lax.psum((grad_wq, grad_wkv), 'sp')  266 us
    ppermute x7, waiting for transfers between devices, body(): lax.ppermute(ring[-1], 'sp', [(dev, (dev + 1) % 8) for dev in range(8)])  51.2 us
    reduce_scatter x1, waiting for transfers between devices, body(): lax.psum_scatter(partial_sums, 'sp', scatter_dimension=0, tiled=True)  48.5 us
    unnamed x132, local copies, waits for them, and re-layouts  25.3 us
    reduce_scatter x1, waiting for transfers between devices, body(): lax.psum_scatter(head_part.astype(jnp.bfloat16), 'dp', scatter_dimension=...  20.8 us
  transfers between devices with their start and end apart: 10, of which 10 were waited for; matrix products, arithmetic and copies ran while one was open for 7% of the time, Pallas kernels for 0%

profile of v1, /device:TPU:0, one launch (start us, length us, event | category | flops | bytes accessed | tf_op | source)
XLA Modules:
  0.0 515.5 jit_solution(11471413862022227911)
XLA Ops:
  16.6 1.7 copy.97
  22.8 3.0 collective-permute-start
  25.8 7.9 %collective-permute-done = bf16[192,512]{1,0:T(8,128)(2,1)S(1)} collective-permute-done((bf16[192,512]{1,0:T(8,128)(2,1)S(1)}, bf16[192,512]{1,0:T(8,128)(2,1)S(1)}, u32[]{:S(2)}, u32[]{:S(2)}) %collective-permute-start) | collective-permute-done | bytes 196640 | tf_op jit(solution)/shard_map/ppermute | solution.py:110
  33.8 1.5 convolution_convert_fusion.1
  35.3 7.3 %collective-permute-done.1 = bf16[192,512]{1,0:T(8,128)(2,1)} collective-permute-done((bf16[192,512]{1,0:T(8,128)(2,1)S(1)}, bf16[192,512]{1,0:T(8,128)(2,1)}, u32[]{:S(2)}, u32[]{:S(2)}) %collective-permute-start.1) | collective-permute-done | bytes 196640 | tf_op jit(solution)/shard_map/ppermute | solution.py:110
  49.5 1.8 collective-permute-done.2
  51.3 8.6 %collective-permute-done.3 = bf16[192,512]{1,0:T(8,128)(2,1)S(1)} collective-permute-done((bf16[192,512]{1,0:T(8,128)(2,1)}, bf16[192,512]{1,0:T(8,128)(2,1)S(1)}, u32[]{:S(2)}, u32[]{:S(2)}) %collective-permute-start.3) | collective-permute-done | bytes 196640 | tf_op jit(solution)/shard_map/ppermute | solution.py:110
  60.0 8.2 %collective-permute-done.4 = bf16[192,512]{1,0:T(8,128)(2,1)S(1)} collective-permute-done((bf16[192,512]{1,0:T(8,128)(2,1)S(1)}, bf16[192,512]{1,0:T(8,128)(2,1)S(1)}, u32[]{:S(2)}, u32[]{:S(2)}) %collective-permute-start.4) | collective-permute-done | bytes 196640 | tf_op jit(solution)/shard_map/ppermute | solution.py:110
  68.3 9.2 %collective-permute-done.5 = bf16[192,512]{1,0:T(8,128)(2,1)S(1)} collective-permute-done((bf16[192,512]{1,0:T(8,128)(2,1)S(1)}, bf16[192,512]{1,0:T(8,128)(2,1)S(1)}, u32[]{:S(2)}, u32[]{:S(2)}) %collective-permute-start.5) | collective-permute-done | bytes 196640 | tf_op jit(solution)/shard_map/ppermute | solution.py:110
  77.8 8.1 %collective-permute-done.6 = bf16[192,512]{1,0:T(8,128)(2,1)S(1)} collective-permute-done((bf16[192,512]{1,0:T(8,128)(2,1)S(1)}, bf16[192,512]{1,0:T(8,128)(2,1)S(1)}, u32[]{:S(2)}, u32[]{:S(2)}) %collective-permute-start.6) | collective-permute-done | bytes 196640 | tf_op jit(solution)/shard_map/ppermute | solution.py:110
  118.3 3.5 copy.117
  124.0 2.0 copy.109
  126.0 1.7 fusion.53
  127.7 1.5 fusion.51
  129.2 1.8 fusion.49
  131.0 1.7 fusion.47
  135.6 1.6 multiply_reduce_fusion
  137.2 2.0 copy.106
  140.9 1.4 multiply_convert_fusion
  142.3 2.8 fusion.160
  145.1 48.5 %reduce-scatter.7.cloned.1.call-done = f32[192,512]{1,0:T(8,128)} async-done(((f32[1536,512]{1,0:T(8,128)}), f32[192,512]{1,0:T(8,128)}) %reduce-scatter.7.cloned.1.call-update) | async-done | bytes 393232 | tf_op jit(solution)/shard_map/reduce_scatter | solution.py:156
  193.6 1.6 slice.225
  195.2 1.8 copy.112
  198.1 1.6 pad_maximum_fusion
  199.7 1.8 copy.113
  202.2 1.7 copy.114
  206.9 2.7 fusion.96
  211.3 1.5 fusion.16
  212.9 266.0 %all-reduce.3.cloned.1.call-done = (f32[512,2048]{1,0:T(8,128)}, f32[512,2048]{1,0:T(8,128)}) async-done(((f32[512,2048]{1,0:T(8,128)}, f32[512,2048]{1,0:T(8,128)}), (f32[512,2048]{1,0:T(8,128)}, f32[512,2048]{1,0:T(8,128)})) %all-reduce.3.cloned.1.call-update) | async-done | bytes 8388624 | tf_op jit(solution)/shard_map/psum | solution.py:179
  478.8 4.7 fusion.146
  483.5 20.8 %reduce-scatter.5.cloned.1.call-done = bf16[192,512]{1,0:T(8,128)(2,1)} async-done(((bf16[192,2048]{1,0:T(8,128)(2,1)}), bf16[192,512]{1,0:T(8,128)(2,1)}) %reduce-scatter.5.cloned.1.call-update) | async-done | bytes 196624 | tf_op jit(solution)/shard_map/reduce_scatter | solution.py:174
  504.3 4.7 copy.159
  (255 shorter events, 65.9 us)
Async XLA Ops:
  7.2 26.6 %copy-start = (bf16[512,2048]{1,0:T(8,128)(2,1)S(1)}, bf16[512,2048]{1,0:T(8,128)(2,1)}, u32[]{:S(2)}) copy-start(bf16[512,2048]{1,0:T(8,128)(2,1)} %param.8) | copy-start | bytes 6291460
  7.2 186.4 %reduce-scatter.7.cloned.1.call-start = ((), (), s32[]{:S(2)}) async-start(), calls=%async_computation.3 | async-start | bytes 3538944 | tf_op jit(solution)/shard_map/reduce_scatter | solution.py:156
  8.1 12.0 %copy-start.46 = (f32[256]{0:T(256)}, f32[256]{0:T(256)S(1)}, u32[]{:S(2)}) copy-start(f32[256]{0:T(256)S(1)} %mul.357) | copy-start | bytes 3076
  9.0 126.1 %copy-start.27 = (f32[192,64]{0,1:T(8,128)}, f32[192,64]{0,1:T(8,128)S(1)}, u32[]{:S(2)}) copy-start(f32[192,64]{0,1:T(8,128)S(1)} %pad_maximum_fusion.5) | copy-start | bytes 147460
  9.1 11.0 %copy-start.23 = (f32[192,256]{1,0:T(8,128)}, f32[192,256]{1,0:T(8,128)S(1)}, u32[]{:S(2)}) copy-start(f32[192,256]{1,0:T(8,128)S(1)} %copy.96) | copy-start | bytes 589828
  14.9 3.5 copy-start.20
  20.2 15.2 %copy-start.25 = (f32[192,256]{1,0:T(8,128)}, f32[192,256]{1,0:T(8,128)S(1)}, u32[]{:S(2)}) copy-start(f32[192,256]{1,0:T(8,128)S(1)} %copy.95) | copy-start | bytes 589828
  22.8 19.8 %copy-start.4 = (bf16[192,512]{1,0:T(8,128)(2,1)S(1)}, bf16[192,512]{1,0:T(8,128)(2,1)}, u32[]{:S(2)}) copy-start(bf16[192,512]{1,0:T(8,128)(2,1)} %param.13) | copy-start | bytes 589828
  22.8 11.0 %collective-permute-start = (bf16[192,512]{1,0:T(8,128)(2,1)S(1)}, bf16[192,512]{1,0:T(8,128)(2,1)S(1)}, u32[]{:S(2)}, u32[]{:S(2)}) collective-permute-start(bf16[192,512]{1,0:T(8,128)(2,1)S(1)} %pad_maximum_fusion.1), channel_id=1, source_target_pairs={{0,4},{4,8},{8,12},{12,16},{16,20},{20,24},{24,28},{28,0},{1,5},{5... | collective-permute-start | bytes 589832 | tf_op jit(solution)/shard_map/ppermute | solution.py:110
  33.8 8.9 %collective-permute-start.1 = (bf16[192,512]{1,0:T(8,128)(2,1)S(1)}, bf16[192,512]{1,0:T(8,128)(2,1)}, u32[]{:S(2)}, u32[]{:S(2)}) collective-permute-start(bf16[192,512]{1,0:T(8,128)(2,1)S(1)} %collective-permute-done), channel_id=1, source_target_pairs={{0,4},{4,8},{8,12},{12,16},{16,20},{20,24},{24,28},{28,0},{1,5},{5... | collective-permute-start | bytes 589832 | tf_op jit(solution)/shard_map/ppermute | solution.py:110
  42.7 8.7 %collective-permute-start.2 = (bf16[192,512]{1,0:T(8,128)(2,1)}, bf16[192,512]{1,0:T(8,128)(2,1)}, u32[]{:S(2)}, u32[]{:S(2)}) collective-permute-start(bf16[192,512]{1,0:T(8,128)(2,1)} %collective-permute-done.1), channel_id=1, source_target_pairs={{0,4},{4,8},{8,12},{12,16},{16,20},{20,24},{24,28},{28,0},{1,5},{5... | collective-permute-start | bytes 589832 | tf_op jit(solution)/shard_map/ppermute | solution.py:110
  42.8 17.1 %copy-start.48 = (f32[64]{0:T(128)S(1)}, f32[64]{0:T(128)}, u32[]{:S(2)}) copy-start(f32[64]{0:T(128)} %param.11) | copy-start | bytes 772
  51.3 8.6 %collective-permute-start.3 = (bf16[192,512]{1,0:T(8,128)(2,1)}, bf16[192,512]{1,0:T(8,128)(2,1)S(1)}, u32[]{:S(2)}, u32[]{:S(2)}) collective-permute-start(bf16[192,512]{1,0:T(8,128)(2,1)} %collective-permute-done.2), channel_id=1, source_target_pairs={{0,4},{4,8},{8,12},{12,16},{16,20},{20,24},{24,28},{28,0},{1,5},{5... | collective-permute-start | bytes 589832 | tf_op jit(solution)/shard_map/ppermute | solution.py:110
  59.9 8.4 %collective-permute-start.4 = (bf16[192,512]{1,0:T(8,128)(2,1)S(1)}, bf16[192,512]{1,0:T(8,128)(2,1)S(1)}, u32[]{:S(2)}, u32[]{:S(2)}) collective-permute-start(bf16[192,512]{1,0:T(8,128)(2,1)S(1)} %collective-permute-done.3), channel_id=1, source_target_pairs={{0,4},{4,8},{8,12},{12,16},{16,20},{20,24},{24,28},{28,0},{1,5},{5... | collective-permute-start | bytes 589832 | tf_op jit(solution)/shard_map/ppermute | solution.py:110
  68.3 9.3 %collective-permute-start.5 = (bf16[192,512]{1,0:T(8,128)(2,1)S(1)}, bf16[192,512]{1,0:T(8,128)(2,1)S(1)}, u32[]{:S(2)}, u32[]{:S(2)}) collective-permute-start(bf16[192,512]{1,0:T(8,128)(2,1)S(1)} %collective-permute-done.4), channel_id=1, source_target_pairs={{0,4},{4,8},{8,12},{12,16},{16,20},{20,24},{24,28},{28,0},{1,5},{5... | collective-permute-start | bytes 589832 | tf_op jit(solution)/shard_map/ppermute | solution.py:110
  77.5 8.4 %collective-permute-start.6 = (bf16[192,512]{1,0:T(8,128)(2,1)S(1)}, bf16[192,512]{1,0:T(8,128)(2,1)S(1)}, u32[]{:S(2)}, u32[]{:S(2)}) collective-permute-start(bf16[192,512]{1,0:T(8,128)(2,1)S(1)} %collective-permute-done.5), channel_id=1, source_target_pairs={{0,4},{4,8},{8,12},{12,16},{16,20},{20,24},{24,28},{28,0},{1,5},{5... | collective-permute-start | bytes 589832 | tf_op jit(solution)/shard_map/ppermute | solution.py:110
  77.8 10.2 %copy-start.37 = (bf16[192,512]{1,0:T(8,128)(2,1)S(1)}, bf16[192,512]{1,0:T(8,128)(2,1)}, u32[]{:S(2)}) copy-start(bf16[192,512]{1,0:T(8,128)(2,1)} %copy-done.36) | copy-start | bytes 589828
  90.0 18.9 %copy-start.1 = (bf16[3072,512]{1,0:T(8,128)(2,1)}, bf16[3072,512]{1,0:T(8,128)(2,1)S(1)}, u32[]{:S(2)}) copy-start(bf16[3072,512]{1,0:T(8,128)(2,1)S(1)} %constant_dynamic-update-slice_fusion.2) | copy-start | bytes 9437188
  97.5 13.2 %copy-start.12 = (bf16[192,1536]{1,0:T(8,128)(2,1)}, bf16[192,1536]{1,0:T(8,128)(2,1)S(1)}, u32[]{:S(2)}) copy-start(bf16[192,1536]{1,0:T(8,128)(2,1)S(1)} %fusion.21) | copy-start | bytes 1769476
  100.4 11.3 %copy-start.13 = (bf16[192,1536]{1,0:T(8,128)(2,1)}, bf16[192,1536]{1,0:T(8,128)(2,1)S(1)}, u32[]{:S(2)}) copy-start(bf16[192,1536]{1,0:T(8,128)(2,1)S(1)} %fusion.19) | copy-start | bytes 1769476
  103.3 9.4 %copy-start.15 = (bf16[192,1536]{1,0:T(8,128)(2,1)}, bf16[192,1536]{1,0:T(8,128)(2,1)S(1)}, u32[]{:S(2)}) copy-start(bf16[192,1536]{1,0:T(8,128)(2,1)S(1)} %fusion.17) | copy-start | bytes 1769476
  106.5 3.3 copy-start.17
  121.8 357.0 %all-reduce.3.cloned.1.call-start = ((), (), s32[]{:S(2)}) async-start(), calls=%async_computation.4 | async-start | bytes 16777216 | tf_op jit(solution)/shard_map/psum | solution.py:179
  126.0 5.0 copy-start.2
  129.2 3.5 copy-start.9
  137.2 3.7 copy-start.50
  145.1 52.9 %copy-start.21 = (f32[192,256]{0,1:T(8,128)S(1)}, f32[192,256]{0,1:T(8,128)}, u32[]{:S(2)}) copy-start(f32[192,256]{0,1:T(8,128)} %copy-done.20) | copy-start | bytes 589828
  145.1 52.9 %copy-start.52 = (f32[64]{0:T(128)S(1)}, f32[64]{0:T(128)}, u32[]{:S(2)}) copy-start(f32[64]{0:T(128)} %param.12) | copy-start | bytes 772
  198.1 6.8 %copy-start.24 = (f32[192,256]{1,0:T(8,128)S(1)}, f32[192,256]{1,0:T(8,128)}, u32[]{:S(2)}) copy-start(f32[192,256]{1,0:T(8,128)} %copy-done.23) | copy-start | bytes 589828
  198.1 6.8 %copy-start.47 = (f32[256]{0:T(256)S(1)}, f32[256]{0:T(256)}, u32[]{:S(2)}) copy-start(f32[256]{0:T(256)} %copy-done.46) | copy-start | bytes 3076
  199.7 5.2 %copy-start.26 = (f32[192,256]{1,0:T(8,128)S(1)}, f32[192,256]{1,0:T(8,128)}, u32[]{:S(2)}) copy-start(f32[192,256]{1,0:T(8,128)} %copy-done.25) | copy-start | bytes 589828
  209.6 294.7 %reduce-scatter.5.cloned.1.call-start = ((), (), s32[]{:S(2)}) async-start(), calls=%async_computation.2 | async-start | bytes 983040 | tf_op jit(solution)/shard_map/reduce_scatter | solution.py:174
  (31 other events, 35.9 us)
Sparse Core Ops, SparseCore 0:
  121.9 71.5 reduce-scatter.6
  209.7 269.0 all-reduce.2
  481.9 22.3 reduce-scatter.4
